TPU v7x, 256 devices: a whole 4x4x8 slice. The times are simulated.
256 devices in a mesh: sp: 32 (over z, x), fs: 4 (over y), tp: 2 (over core).
Axes of the slice: x: 4, y: 4, z: 8, core: 2. Of those that a mesh axis runs over, the one named last changes fastest.
Arguments:
- tokens: bfloat16 [4, 4096, 2048], P('fs', 'sp', 'tp'), may hold values from -6 to 6
- norm_gain: float32 [2048], replicated, may hold values from 0.1 to 1.9
- conv_gate_out: bfloat16 [2048, 512], P(('sp', 'fs'), 'tp'), may hold values from -0.125 to 0.125
- conv_gate_in: bfloat16 [2048, 512], P(('sp', 'fs'), 'tp'), may hold values from -0.125 to 0.125
- conv_value: bfloat16 [2048, 512], P(('sp', 'fs'), 'tp'), may hold values from -0.125 to 0.125
- conv_taps: float32 [3, 512], P(None, 'tp'), may hold values from -3.5 to 3.5
- recv_weight: bfloat16 [2048, 512], P(('sp', 'fs'), 'tp'), may hold values from -0.125 to 0.125
- key_weight: bfloat16 [2048, 512], P(('sp', 'fs'), 'tp'), may hold values from -0.125 to 0.125
- value_weight: bfloat16 [2048, 512], P(('sp', 'fs'), 'tp'), may hold values from -0.125 to 0.125
- decay_base: float32 [512], P('tp'), may hold values from -12.5 to -3.3
- decay_down: bfloat16 [2048, 64], replicated, may hold values from -0.125 to 0.125
- decay_up: bfloat16 [64, 512], P(None, 'tp'), may hold values from -1.5 to 1.5
- decay_shift: float32 [4, 4096, 8], P('fs', 'sp', 'tp'), may hold values from -0.7 to 11.5
- rate_base: float32 [512], P('tp'), may hold values from -4 to 4
- rate_down: bfloat16 [2048, 64], replicated, may hold values from -0.125 to 0.125
- rate_up: bfloat16 [64, 512], P(None, 'tp'), may hold values from -0.75 to 0.75
- head_gain: float32 [512], P('tp'), may hold values from 0.1 to 1.9
- out_conv: bfloat16 [512, 2048], P('tp', ('sp', 'fs')), may hold values from -0.1875 to 0.1875
- out_state: bfloat16 [512, 2048], P('tp', ('sp', 'fs')), may hold values from -0.1875 to 0.1875
Outputs:
- mixed_out: bfloat16 [4, 4096, 2048], P('fs', ('sp', 'tp'))
All inputs are finite; a program needn't handle non-finite values.
Results may differ from a plain program's by a relative error of at most 0.015.
Values may be sent and summed in bfloat16 or wider, within the bound.
A program may use at most 64 MiB of HBM per device.

v0:
```python
from functools import partial
import math

import jax
import jax.numpy as jnp
from jax import lax
from jax.sharding import Mesh
from jax.sharding import PartitionSpec as P

SP = ("sp_0", "sp_1")
SP_FS = ("sp_0", "sp_1", "fs")
SP_TP = ("sp_0", "sp_1", "tp")


RMS_EPS = 1e-05
GROUP_EPS = 0.00064
UNIT_EPS = 1e-06


def laid_out(pieces, dim):
    pieces = jnp.moveaxis(pieces, 0, dim)
    shape = pieces.shape
    return pieces.reshape(*shape[:dim], shape[dim] * shape[dim + 1], *shape[dim + 2 :])


def sent_to_all(array, axis):
    copies = jnp.broadcast_to(array, (lax.axis_size(axis), *array.shape))
    return lax.all_to_all(copies, axis, split_axis=0, concat_axis=0, tiled=True)


def gather_directly(array, axis, dim):
    return laid_out(sent_to_all(array, axis), dim)


def in_one_piece(arrays, axis, dim, along):
    widths = [a.shape[along] for a in arrays]
    both = jnp.concatenate(arrays, axis=along)
    result = lax.all_gather(both, axis, axis=dim, tiled=True)
    return tuple(jnp.split(result, [sum(widths[:k]) for k in range(1, len(widths))], axis=along))


def from_behind(array, axis, by):
    size = lax.axis_size(axis)
    pairs = [(i, i + by) for i in range(size) if 0 <= i + by < size]
    return lax.ppermute(array, axis, pairs)


def filled_with(array, identity):
    return jax.tree.map(
        lambda a, e: jnp.broadcast_to(jnp.asarray(e, a.dtype), a.shape), array, identity
    )


def entering_2(array, axes, combine, identity):
    before = start = filled_with(array, identity)
    subtotal = array
    for axis in reversed(axes):
        size, index = (lax.axis_size(axis), lax.axis_index(axis))
        pieces = jax.tree.map(
            lambda part, kind: lax.all_gather(part.astype(kind), axis),
            subtotal,
            (jnp.bfloat16, jnp.bfloat16),
        )
        inside, subtotal = (start, start)
        for k in range(size):
            passed = k < index
            subtotal = combine(
                subtotal, jax.tree.map(lambda part, own: part[k].astype(own.dtype), pieces, array)
            )
            inside = jax.tree.map(lambda new, old: jnp.where(passed, new, old), subtotal, inside)
        before = combine(inside, before)
    return before


def gather_turned(arrays, axis, dims):
    turned = [jnp.moveaxis(a, dim, 0) for a, dim in zip(arrays, dims)]
    widths = [t[0].size for t in turned]
    both = jnp.concatenate([t.reshape(-1, w) for t, w in zip(turned, widths)], axis=1)
    result = lax.all_gather(both, axis, axis=0, tiled=True)
    pieces = jnp.split(result, [sum(widths[:k]) for k in range(1, len(widths))], axis=1)
    return tuple(
        (
            jnp.moveaxis(b.reshape(-1, *t.shape[1:]), 0, dim)
            for b, t, dim in zip(pieces, turned, dims)
        )
    )


def in_blocks(array, dim, size):
    shape = array.shape
    pieces = array.reshape(*shape[:dim], size, shape[dim] // size, *shape[dim + 1 :])
    return jnp.moveaxis(pieces, dim, 0)


def sum_at_owner(array, axis, dim):
    pieces = in_blocks(array, dim, lax.axis_size(axis))
    arrived = lax.all_to_all(pieces, axis, split_axis=0, concat_axis=0, tiled=True)
    return arrived.astype(jnp.float32).sum(axis=0)


def fold_rows(normed, totals, pieces, offset):
    return tuple(
        (
            jnp.dot(normed, pieces[member], preferred_element_type=jnp.float32)
            for member in range(len(pieces))
        )
    )


def block_step(carried, inputs):
    log_dec, remove_dir, write_dir, key_rate, receive, val_rows = inputs
    cumulative = jnp.cumsum(log_dec, axis=1)
    exclusive = cumulative - log_dec
    length = log_dec.shape[1]
    where_t = lax.broadcasted_iota(jnp.int32, (length, length), 0)
    where_s = lax.broadcasted_iota(jnp.int32, (length, length), 1)
    strict = (where_t > where_s)[None, :, :, None]
    inclusive = (where_t >= where_s)[None, :, :, None]
    damp_prior = jnp.where(
        strict, jnp.exp(jnp.minimum(exclusive[:, :, None, :] - cumulative[:, None, :, :], 0.0)), 0.0
    )
    damp_now = jnp.where(
        inclusive,
        jnp.exp(jnp.minimum(cumulative[:, :, None, :] - cumulative[:, None, :, :], 0.0)),
        0.0,
    )
    link_ab = jnp.einsum("htc,htsc,hsc->hts", remove_dir, damp_prior, write_dir)
    link_ak = jnp.einsum("htc,htsc,hsc->hts", remove_dir, damp_prior, key_rate)
    from_start = jnp.einsum("hrc,htc->htr", carried, remove_dir * jnp.exp(exclusive))
    rhs_terms = from_start + jnp.einsum("hts,hsr->htr", link_ak, val_rows)
    unit_matrix = jnp.eye(length, dtype=jnp.float32)
    projected = lax.linalg.triangular_solve(
        unit_matrix - link_ab, rhs_terms, left_side=True, lower=True, unit_diagonal=True
    )
    read_b = jnp.einsum("htc,htsc,hsc->hts", receive, damp_now, write_dir)
    read_k = jnp.einsum("htc,htsc,hsc->hts", receive, damp_now, key_rate)
    outputs = (
        jnp.einsum("hrc,htc->htr", carried, receive * jnp.exp(cumulative))
        + jnp.einsum("hts,hsr->htr", read_b, projected)
        + jnp.einsum("hts,hsr->htr", read_k, val_rows)
    )
    to_end = jnp.exp(cumulative[:, -1:, :] - cumulative)
    new_state = (
        carried * jnp.exp(cumulative[:, -1, :])[:, None, :]
        + jnp.einsum("hsr,hsc->hrc", projected, write_dir * to_end)
        + jnp.einsum("hsr,hsc->hrc", val_rows, key_rate * to_end)
    )
    return (new_state, outputs)


def compose(earlier, later):
    return (
        jnp.einsum("hij,hjk->hik", earlier[0], later[0]),
        jnp.einsum("hij,hjk->hik", earlier[1], later[0]) + later[1],
    )


def body(
    tokens,
    norm_gain,
    conv_gate_out,
    conv_gate_in,
    conv_value,
    conv_taps,
    recv_weight,
    key_weight,
    value_weight,
    decay_base,
    decay_down,
    decay_up,
    decay_shift,
    rate_base,
    rate_down,
    rate_up,
    head_gain,
    out_conv,
    out_state,
):
    tok_count = tokens.shape[1]
    own_half = tokens.reshape(tok_count, tokens.shape[2])
    features = gather_directly(own_half, "tp", 1).astype(jnp.float32)
    normed = (
        features
        * lax.rsqrt(jnp.mean(features * features, axis=-1, keepdims=True) + RMS_EPS)
        * norm_gain
    ).astype(jnp.bfloat16)
    widths = (
        conv_gate_out.shape[1],
        conv_gate_in.shape[1],
        conv_value.shape[1],
        recv_weight.shape[1],
        key_weight.shape[1],
        value_weight.shape[1],
    )
    zeros_init = tuple(
        (jnp.zeros((tok_count, column_count), jnp.float32) for column_count in widths)
    )
    row_adder = partial(fold_rows, normed)
    local_go, local_gi, local_cv, local_rw, local_kw, local_vw = in_one_piece(
        (conv_gate_out, conv_gate_in, conv_value, recv_weight, key_weight, value_weight), "fs", 0, 1
    )
    projected_sums = row_adder(
        zeros_init,
        in_one_piece((local_go, local_gi, local_cv, local_rw, local_kw, local_vw), SP, 0, 1),
        jnp.int32(0),
    )
    gate_out, gate_in, conv_in, recv_raw, keys_raw, vals_raw = tuple(
        (member.astype(jnp.bfloat16) for member in projected_sums)
    )
    mixed_in = gate_in.astype(jnp.float32) * conv_in.astype(jnp.float32)
    edge_rows = from_behind(mixed_in[-2:], SP, 1)
    padded = jnp.concatenate([edge_rows, mixed_in], axis=0)
    convolved = (
        padded[0:tok_count] * conv_taps[0]
        + padded[1 : tok_count + 1] * conv_taps[1]
        + padded[2:] * conv_taps[2]
    )
    conv_out = (gate_out.astype(jnp.float32) * convolved).astype(jnp.bfloat16)
    heads_here = decay_shift.shape[2]
    head_size = recv_raw.shape[1] // heads_here
    shaped = (tok_count, heads_here, head_size)
    decay_low = jnp.tanh(jnp.dot(normed, decay_down, preferred_element_type=jnp.float32)).astype(
        jnp.bfloat16
    )
    rate_low = jnp.dot(normed, rate_down, preferred_element_type=jnp.float32).astype(jnp.bfloat16)
    decay_pre = decay_base + jnp.dot(decay_low, decay_up, preferred_element_type=jnp.float32)
    log_base = -jax.nn.softplus(-decay_pre) - 0.5
    log_decay = -jnp.exp(log_base.reshape(shaped) + decay_shift.reshape(tok_count, heads_here, 1))
    learn_rate = jax.nn.sigmoid(
        rate_base + jnp.dot(rate_low, rate_up, preferred_element_type=jnp.float32)
    ).reshape(shaped)
    keys_float = keys_raw.astype(jnp.float32).reshape(shaped)
    unit_keys = keys_float * lax.rsqrt(
        jnp.sum(keys_float * keys_float, axis=-1, keepdims=True) + UNIT_EPS
    )
    values_float = vals_raw.astype(jnp.float32).reshape(shaped)
    recv_float = recv_raw.astype(jnp.float32).reshape(shaped)
    block_len = math.gcd(tok_count, 32)
    blocks = tok_count // block_len

    def to_blocks(field):
        return field.reshape(blocks, block_len, heads_here, field.shape[2]).transpose(0, 2, 1, 3)

    val_rows = jnp.concatenate([values_float, jnp.zeros_like(values_float)], axis=2)
    basis = jnp.broadcast_to(
        jnp.eye(head_size, dtype=jnp.float32), (heads_here, head_size, head_size)
    )
    empty_rows = jnp.zeros((heads_here, head_size, head_size), jnp.float32)
    start_rows = jnp.concatenate([empty_rows, basis], axis=1)
    end_rows, outputs = lax.scan(
        block_step,
        start_rows,
        (
            to_blocks(log_decay),
            to_blocks(-unit_keys),
            to_blocks(unit_keys * learn_rate),
            to_blocks(keys_float * learn_rate),
            to_blocks(recv_float),
            to_blocks(val_rows),
        ),
    )
    offset_part = end_rows[:, :head_size, :]
    transit = end_rows[:, head_size:, :]
    prefix = entering_2((transit, offset_part), SP, compose, (basis, empty_rows))
    entering = prefix[1]
    direct = outputs[..., :head_size]
    through = outputs[..., head_size:]
    state_read = direct + jnp.einsum("hji,nhti->nhtj", entering, through)
    state_read = state_read.transpose(0, 2, 1, 3).reshape(shaped)
    centre = jnp.mean(state_read, axis=-1, keepdims=True)
    centred = state_read - centre
    variance = jnp.mean(centred * centred, axis=-1, keepdims=True)
    state_out = (
        (centred * lax.rsqrt(variance + GROUP_EPS)).reshape(tok_count, heads_here * head_size)
        * head_gain
    ).astype(jnp.bfloat16)
    local_oc, local_os = gather_turned((out_conv, out_state), "fs", (1, 1))
    conv_cols, state_cols = gather_turned((local_oc, local_os), SP, (1, 1))
    tp_count = lax.axis_size("tp")
    own_rows = tok_count // tp_count
    merged = sum_at_owner(
        (
            jnp.dot(conv_out, conv_cols, preferred_element_type=jnp.float32)
            + jnp.dot(state_out, state_cols, preferred_element_type=jnp.float32)
        ).astype(jnp.bfloat16),
        "tp",
        0,
    )
    return merged.astype(jnp.bfloat16).reshape(1, own_rows, merged.shape[1])


def solution(mesh):
    torus = Mesh(
        mesh.devices.reshape(8, 4, mesh.shape["fs"], mesh.shape["tp"]), ("sp_0", "sp_1", "fs", "tp")
    )
    placed = (
        P("fs", SP, "tp"),
        P(),
        P(SP_FS, "tp"),
        P(SP_FS, "tp"),
        P(SP_FS, "tp"),
        P(None, "tp"),
        P(SP_FS, "tp"),
        P(SP_FS, "tp"),
        P(SP_FS, "tp"),
        P("tp"),
        P(),
        P(None, "tp"),
        P("fs", SP, "tp"),
        P("tp"),
        P(),
        P(None, "tp"),
        P("tp"),
        P("tp", SP_FS),
        P("tp", SP_FS),
    )
    return jax.shard_map(
        body, mesh=torus, in_specs=placed, out_specs=P("fs", SP_TP, None), check_vma=False
    )
```

profile of v0, /device:TPU:1, one launch (start us, length us, event | category | flops | bytes accessed | tf_op | source)
XLA Modules:
  0.0 286.1 jit_solution(4917845523079927253)
XLA Ops:
  10.8 11.6 %all_gather.36 = bf16[64,1536]{1,0:T(8,128)(2,1)} all-gather(bf16[16,1536]{1,0:T(8,128)(2,1)S(1)} %constant_dynamic-update-slice_fusion), channel_id=1, replica_groups=mesh['sp_0'=8,'sp_1'=4,'fs'=4,'tp'=2] {'fs'}, dimensions={0}, use_global_device_ids=true | all-gather | bytes 245760 | tf_op jit(solution)/shard_map/all_gather | solution.py:38
  22.5 1.1 copy.56
  24.5 8.0 %all-to-all-start = ((bf16[2,128,1024]{1,2,0:T(8,128)(2,1)}), bf16[2,128,1024]{1,2,0:T(8,128)(2,1)S(1)}, u32[]{:S(2)}, u32[]{:S(2)}) async-start(bf16[2,128,1024]{1,2,0:T(8,128)(2,1)} %broadcast_in_dim.57), calls=%async_computation | async-start | bytes 1048576 | tf_op jit(solution)/shard_map/all_to_all | solution.py:28
  32.5 9.7 %all_gather.38 = bf16[64,512]{1,0:T(8,128)(2,1)} all-gather(bf16[16,512]{1,0:T(8,128)(2,1)S(1)} %pad_maximum_fusion.1), channel_id=1, replica_groups=mesh['sp_0'=8,'sp_1'=4,'fs'=4,'tp'=2] {'fs'}, dimensions={0}, use_global_device_ids=true | all-gather | bytes 81920 | tf_op jit(solution)/shard_map/all_gather | solution.py:79
  44.7 70.2 %all-gather.7.cloned.1.call-done = bf16[2048,1536]{1,0:T(8,128)(2,1)} async-done(((bf16[64,1536]{1,0:T(8,128)(2,1)}), bf16[2048,1536]{1,0:T(8,128)(2,1)}) %all-gather.7.cloned.1.call-update) | async-done | bytes 6291472 | tf_op jit(solution)/shard_map/all_gather | solution.py:38
  114.8 1.6 fusion.193
  116.8 1.6 fusion.73
  118.5 1.6 convolution_convert_fusion.1
  120.7 62.2 %while.12 = (s32[]{:T(128)}, f32[4,128,64]{1,2,0:T(8,128)S(1)}, f32[4,4,32,128]{3,2,0,1:T(8,128)S(1)}, f32[4,4,32,64]{3,2,1,0:T(8,128)S(1)}, f32[4,4,32,64]{3,2,...) while((s32[]{:T(128)}, f32[4,128,64]{1,2,0:T(8,128)S(1)}, ...), condition=%wide.region_4.5_spmd, body=%wide.region_2.4_spmd.sunk | while | flops 24595488 | bytes 3147141 | solution.py:250
  120.9 1.0 fusion.292
  122.0 9.9 %custom-call.7 = f32[4,1,32,32]{2,3,1,0:T(8,128)S(1)} custom-call(f32[4,1,32,32]{3,2,1,0:T(8,128)S(1)} %add_bitcast_fusion.2), custom_call_target="InvertDiagBlocksLowerTriangular" | custom-call | tf_op jit(solution)/shard_map/while/body/eval_jaxpr/triangular_solve | solution.py:132
  131.9 1.0 fusion.291
  134.7 1.0 fusion.298
  137.6 9.9 %custom-call.7 = f32[4,1,32,32]{2,3,1,0:T(8,128)S(1)} custom-call(f32[4,1,32,32]{3,2,1,0:T(8,128)S(1)} %add_bitcast_fusion.2), custom_call_target="InvertDiagBlocksLowerTriangular" | custom-call | tf_op jit(solution)/shard_map/while/body/eval_jaxpr/triangular_solve | solution.py:132
  149.0 1.0 fusion.297
  153.1 9.8 %custom-call.7 = f32[4,1,32,32]{2,3,1,0:T(8,128)S(1)} custom-call(f32[4,1,32,32]{3,2,1,0:T(8,128)S(1)} %add_bitcast_fusion.2), custom_call_target="InvertDiagBlocksLowerTriangular" | custom-call | tf_op jit(solution)/shard_map/while/body/eval_jaxpr/triangular_solve | solution.py:132
  162.9 1.0 fusion.291
  165.8 1.0 fusion.298
  167.6 1.0 fusion.292
  168.6 9.8 %custom-call.7 = f32[4,1,32,32]{2,3,1,0:T(8,128)S(1)} custom-call(f32[4,1,32,32]{3,2,1,0:T(8,128)S(1)} %add_bitcast_fusion.2), custom_call_target="InvertDiagBlocksLowerTriangular" | custom-call | tf_op jit(solution)/shard_map/while/body/eval_jaxpr/triangular_solve | solution.py:132
  178.5 1.0 fusion.291
  181.3 1.0 fusion.298
  183.1 10.6 %all-gather = bf16[16,64,64]{2,1,0:T(8,128)(2,1)S(1)} all-gather(bf16[4,64,64]{2,1,0:T(8,128)(2,1)S(1)} %get-tuple-element.111), channel_id=2, replica_groups=mesh['sp_0'=8,'sp_1'=4,'fs'=4,'tp'=2] {'sp_1'}, dimensions={0}, use_global_device_ids=true | all-gather | bytes 163840 | tf_op jit(solution)/shard_map/all_gather | solution.py:60
  194.1 1.6 fusion.77
  195.6 1.6 fusion.76
  197.4 1.6 collective-permute-start
  199.0 9.8 %all-gather.2 = bf16[16,64,64]{2,1,0:T(8,128)(2,1)S(1)} all-gather(bf16[4,64,64]{2,1,0:T(8,128)(2,1)S(1)} %get-tuple-element.112), channel_id=4, replica_groups=mesh['sp_0'=8,'sp_1'=4,'fs'=4,'tp'=2] {'sp_1'}, dimensions={0}, use_global_device_ids=true | all-gather | bytes 163840 | tf_op jit(solution)/shard_map/all_gather | solution.py:60
  208.8 20.0 %all-gather.1 = bf16[32,64,64]{2,1,0:T(8,128)(2,1)S(1)} all-gather(bf16[4,64,64]{2,1,0:T(8,128)(2,1)S(1)} %fusion.173), channel_id=3, replica_groups=mesh['sp_0'=8,'sp_1'=4,'fs'=4,'tp'=2] {'sp_0'}, dimensions={0}, use_global_device_ids=true | all-gather | bytes 294912 | tf_op jit(solution)/shard_map/all_gather | solution.py:60
  229.4 20.0 %all-gather.3 = bf16[32,64,64]{2,1,0:T(8,128)(2,1)S(1)} all-gather(bf16[4,64,64]{2,1,0:T(8,128)(2,1)S(1)} %convolution_add_fusion.13), channel_id=5, replica_groups=mesh['sp_0'=8,'sp_1'=4,'fs'=4,'tp'=2] {'sp_0'}, dimensions={0}, use_global_device_ids=true | all-gather | bytes 294912 | tf_op jit(solution)/shard_map/all_gather | solution.py:60
  252.4 2.5 fusion.84
  254.9 1.7 fusion.59
  256.7 21.8 %all_to_all.10 = bf16[2,64,2048]{2,1,0:T(8,128)(2,1)S(1)} all-to-all(bf16[2,64,2048]{2,1,0:T(8,128)(2,1)S(1)} %bitcast.234), channel_id=1, replica_groups=mesh['sp_0'=8,'sp_1'=4,'fs'=4,'tp'=2] {'tp'}, dimensions={0} | all-to-all | bytes 1048576 | tf_op jit(solution)/shard_map/all_to_all | solution.py:97
  (186 shorter events, 27.2 us)
Async XLA Ops:
  6.5 36.5 %copy-start = (bf16[2048,64]{0,1:T(8,128)(2,1)S(1)}, bf16[2048,64]{0,1:T(8,128)(2,1)}, u32[]{:S(2)}) copy-start(bf16[2048,64]{0,1:T(8,128)(2,1)} %param.35) | copy-start | bytes 786436
  6.5 26.0 %copy-start.5 = (bf16[256,16]{0,1:T(8,128)(2,1)S(1)}, bf16[256,16]{0,1:T(8,128)(2,1)}, u32[]{:S(2)}) copy-start(bf16[256,16]{0,1:T(8,128)(2,1)} %param.38) | copy-start | bytes 24580
  6.5 26.0 %copy-start.4 = (bf16[256,16]{0,1:T(8,128)(2,1)S(1)}, bf16[256,16]{0,1:T(8,128)(2,1)}, u32[]{:S(2)}) copy-start(bf16[256,16]{0,1:T(8,128)(2,1)} %param.39) | copy-start | bytes 24580
  6.5 36.1 %copy-start.3 = (f32[2048]{0:T(1024)S(1)}, f32[2048]{0:T(1024)}, u32[]{:S(2)}) copy-start(f32[2048]{0:T(1024)} %param.22) | copy-start | bytes 24580
  6.5 108.3 %all-gather.7.cloned.1.call-start = ((), (), s32[]{:S(2)}) async-start(), calls=%async_computation.2 | async-start | bytes 6488064 | tf_op jit(solution)/shard_map/all_gather | solution.py:38
  22.5 20.5 %copy-start.10 = (bf16[64,256]{1,0:T(8,128)(2,1)S(1)}, bf16[64,256]{1,0:T(8,128)(2,1)}, u32[]{:S(2)}) copy-start(bf16[64,256]{1,0:T(8,128)(2,1)} %param.36) | copy-start | bytes 98308
  22.5 20.5 %copy-start.11 = (f32[256]{0:T(256)S(1)}, f32[256]{0:T(256)}, u32[]{:S(2)}) copy-start(f32[256]{0:T(256)} %param.34) | copy-start | bytes 3076
  24.5 19.1 %copy-start.1 = (bf16[2048,64]{0,1:T(8,128)(2,1)S(1)}, bf16[2048,64]{0,1:T(8,128)(2,1)}, u32[]{:S(2)}) copy-start(bf16[2048,64]{0,1:T(8,128)(2,1)} %param.31) | copy-start | bytes 786436
  24.5 19.2 %copy-start.2 = (bf16[64,256]{1,0:T(8,128)(2,1)S(1)}, bf16[64,256]{1,0:T(8,128)(2,1)}, u32[]{:S(2)}) copy-start(bf16[64,256]{1,0:T(8,128)(2,1)} %param.32) | copy-start | bytes 98308
  24.5 19.2 %copy-start.8 = (f32[256]{0:T(256)S(1)}, f32[256]{0:T(256)}, u32[]{:S(2)}) copy-start(f32[256]{0:T(256)} %param.30) | copy-start | bytes 3076
  24.5 17.8 %all-to-all-start = ((bf16[2,128,1024]{1,2,0:T(8,128)(2,1)}), bf16[2,128,1024]{1,2,0:T(8,128)(2,1)S(1)}, u32[]{:S(2)}, u32[]{:S(2)}) async-start(bf16[2,128,1024]{1,2,0:T(8,128)(2,1)} %broadcast_in_dim.57), calls=%async_computation | async-start | bytes 1048576 | tf_op jit(solution)/shard_map/all_to_all | solution.py:28
  32.5 219.9 %all-gather.9.cloned.1.call-start = ((), (), s32[]{:S(2)}) async-start(), calls=%async_computation.3 | async-start | bytes 2162688 | tf_op jit(solution)/shard_map/all_gather | solution.py:79
  42.3 2.0 copy-start.7
  42.6 1.9 copy-start.6
  197.4 55.1 %collective-permute-start = (f32[2,256]{1,0:T(2,128)S(1)}, f32[2,256]{1,0:T(2,128)S(1)}, u32[]{:S(2)}, u32[]{:S(2)}) collective-permute-start(f32[2,256]{1,0:T(2,128)S(1)} %slice.173), channel_id=1, source_target_pairs={{0,8},{8,16},{16,24},{24,32},{32,40},{40,48},{48,56},{56,64},{64,7... | collective-permute-start | bytes 6152 | tf_op jit(solution)/shard_map/ppermute | solution.py:45
  252.3 2.7 copy-start.9
Sparse Core Ops, SparseCore 0:
  22.6 92.1 all-gather.6
  117.4 73.0 all-gather.8
where the time goes:
time: 287 us; the launch traced here: 286 us
  blocking collectives  104 us (36%)
  waiting for transfers between devices  70.2 us (24%)
  other arithmetic  42.4 us (15%)
  matrix products  37.3 us (13%)
  between operations  13.9 us (5%)
  starting transfers between devices  9.69 us (3%)
  local copies, waits for them, and re-layouts  8.72 us (3%)
    all_gather x1, waiting for transfers between devices, in_one_piece(): result = lax.all_gather(both, axis, axis=dim, tiled=True)  70.2 us
    all_gather x4, blocking collectives, entering_2(): lax.all_gather(part.astype(kind), axis)  60.4 us
    another operation x20, other arithmetic, block_step(): lax.linalg.triangular_solve(unit_matrix - link_ab, rhs_terms, left_side=T...  39.9 us
    all_to_all x1, blocking collectives, sum_at_owner(): lax.all_to_all(pieces, axis, split_axis=0, concat_axis=0, tiled=True)  21.8 us
    all_gather x1, blocking collectives, in_one_piece(): result = lax.all_gather(both, axis, axis=dim, tiled=True)  11.6 us
    all_gather x1, blocking collectives, gather_turned(): result = lax.all_gather(both, axis, axis=0, tiled=True)  9.71 us
    all_to_all x1, starting transfers between devices, sent_to_all(): return lax.all_to_all(copies, axis, split_axis=0, concat_axis=0, tiled=True)  8.02 us
    dot_general x5, matrix products, fold_rows(): jnp.dot(normed, pieces[member], preferred_element_type=jnp.float32)  7.87 us
  transfers between devices with their start and end apart: 4, of which 1 were waited for; matrix products, arithmetic and copies ran while one was open for 28% of the time, Pallas kernels for 0%

commit v1 on v0

v1 whole, which is shorter than its diff:
```python
import functools

import jax
import jax.numpy as jnp
from jax import lax
from jax.experimental import pallas as pl
from jax.experimental.pallas import tpu as pltpu
from jax.sharding import Mesh
from jax.sharding import PartitionSpec as P

SP = ("sp_0", "sp_1")
SP_FS = ("sp_0", "sp_1", "fs")
SP_TP = ("sp_0", "sp_1", "tp")
BF = jnp.bfloat16
F32 = jnp.float32
RMS_EPS = 1e-05
GROUP_EPS = 0.00064
UNIT_EPS = 1e-06
T = 128
HD = 64
NZ, NX, NY = 8, 4, 4
MESH = pl.DeviceIdType.MESH
VM = pltpu.VMEM


def at_axis(name, index):
    return {name: index}


class Copies:
    def __init__(self, send_sems, recv_sems):
        self.send_sems, self.recv_sems = send_sems, recv_sems
        self.used = 0
        self.sent = []

    def slot(self):
        self.used += 1
        return self.used - 1

    def make(self, slot, src, dst, where):
        return pltpu.make_async_remote_copy(
            src_ref=src,
            dst_ref=dst,
            send_sem=self.send_sems.at[slot],
            recv_sem=self.recv_sems.at[slot],
            device_id=where,
            device_id_type=MESH,
        )

    def send(self, slot, src, dst, where):
        copy = self.make(slot, src, dst, where)
        copy.start()
        self.sent.append(copy)

    def arrived(self, slot, ref, where):
        self.make(slot, ref, ref, where).wait_recv()

    def finish(self):
        for copy in self.sent:
            copy.wait_send()


def gather_kernel(
    tok, wsl, own, shift, tok_all, w_all, o_slab, sh_all, w_own, local_sems, send_sems, recv_sems
):
    z, x = lax.axis_index("sp_0"), lax.axis_index("sp_1")
    y, c = lax.axis_index("fs"), lax.axis_index("tp")

    def up(i, by, n):
        return lax.rem(i + by + n, n)

    locals_ = [
        pltpu.make_async_copy(tok, tok_all.at[x, c], local_sems.at[0]),
        pltpu.make_async_copy(wsl, w_own, local_sems.at[1]),
        pltpu.make_async_copy(wsl.at[x], w_all.at[z, x, y], local_sems.at[2]),
        pltpu.make_async_copy(own, o_slab.at[z, y], local_sems.at[3]),
        pltpu.make_async_copy(shift, sh_all.at[x], local_sems.at[4]),
    ]
    for copy in locals_:
        copy.start()
    barrier = pltpu.get_barrier_semaphore()
    peers = [at_axis("sp_1", up(x, d, NX)) for d in (1, 2, 3)]
    peers += [at_axis("fs", up(y, d, NY)) for d in (1, 2, 3)]
    peers += [at_axis("sp_0", up(z, 1, NZ)), at_axis("sp_0", up(z, -1, NZ))]
    peers += [at_axis("tp", 1 - c)]
    for peer in peers:
        pl.semaphore_signal(barrier, inc=1, device_id=peer, device_id_type=MESH)
    pl.semaphore_wait(barrier, len(peers))
    for copy in locals_:
        copy.wait()

    net = Copies(send_sems, recv_sems)
    todo = []
    right, left = at_axis("sp_1", up(x, 1, NX)), at_axis("sp_1", up(x, -1, NX))
    partner = at_axis("tp", 1 - c)

    in_slots = [None] + [net.slot() for _ in range(3)]
    sh_slots = [None] + [net.slot() for _ in range(3)]
    for d in (1, 2, 3):
        to = up(x, d, NX)
        net.send(in_slots[d], w_own.at[to], w_all.at[z, x, y], at_axis("sp_1", to))
    for d in (1, 2, 3):
        net.send(sh_slots[d], sh_all.at[x], sh_all.at[x], at_axis("sp_1", up(x, d, NX)))

    zr, zl = at_axis("sp_0", up(z, 1, NZ)), at_axis("sp_0", up(z, -1, NZ))

    def z_ring(view, parts, ready, start, step):
        slots = {}
        half = parts // 2
        for k in range(1, 5):
            for way in (1, -1):
                for e in range(parts):
                    if k < 4 or (e < half) == (way == 1):
                        slots[way, k, e] = net.slot()
        for k in range(1, 5):
            for e in range(parts):

                def act(k=k, e=e):
                    if k == 1:
                        ready(e)
                    for way, nxt in ((1, zr), (-1, zl)):
                        ref = view(up(z, way * (1 - k), NZ), e)
                        if k > 1:
                            net.arrived(slots[way, k - 1, e], ref, nxt)
                        if (way, k, e) in slots:
                            net.send(slots[way, k, e], ref, ref, nxt)

                todo.append((start + step * (k - 1) + 0.01 * e, act))

        def last():
            for way, nxt in ((1, zr), (-1, zl)):
                for e in range(parts):
                    if (way, 4, e) in slots:
                        net.arrived(slots[way, 4, e], view(up(z, -4, NZ), e), nxt)

        todo.append((start + step * 4, last))

    z_ring(lambda i, e: o_slab.at[i, y, pl.ds(8 * e, 8)], 2, lambda e: None, 0.5, 2.2)

    yr, yl = at_axis("fs", up(y, 1, NY)), at_axis("fs", up(y, -1, NY))
    y_slots = {(way, k, h): net.slot() for way in (1, -1) for k in (1, 2) for h in (0, 1)
               if k == 1 or (h == 0) == (way == 1)}

    def o_view(i, h):
        return o_slab.at[pl.ds(4 * h, 4), i]

    def o_first():
        for way, nxt in ((1, yr), (-1, yl)):
            for h in (0, 1) if way == 1 else (1, 0):
                net.send(y_slots[way, 1, h], o_view(y, h), o_view(y, h), nxt)

    def o_second():
        for way, nxt in ((1, yr), (-1, yl)):
            h = 0 if way == 1 else 1
            ref = o_view(up(y, -way, NY), h)
            net.arrived(y_slots[way, 1, h], ref, nxt)
            net.send(y_slots[way, 2, h], ref, ref, nxt)

    def o_last():
        for way, nxt in ((1, yr), (-1, yl)):
            h = 0 if way == 1 else 1
            ref = o_view(up(y, -way, NY), 1 - h)
            net.arrived(y_slots[way, 1, 1 - h], ref, nxt)
            ref = o_view(up(y, 2, NY), h)
            net.arrived(y_slots[way, 2, h], ref, nxt)

    todo += [(9.4, o_first), (13.0, o_second), (17.0, o_last)]

    tok_slots = {(way, k, h): net.slot() for way in (1, -1) for k in (1, 2) for h in (0, 1)
                 if k == 1 or (h == 0) == (way == 1)}
    chip_slots = {(d, h): net.slot() for d in range(4) for h in (0, 1)}

    def t_view(i, h, core=None):
        return tok_all.at[i, c if core is None else core, pl.ds(64 * h, 64)]

    def across(d, h):
        ref = t_view(up(x, d, NX), h)
        net.send(chip_slots[d, h], ref, ref, partner)

    def t_first():
        for h in (0, 1):
            for way, nxt in ((1, right), (-1, left)):
                g = h if way == 1 else 1 - h
                net.send(tok_slots[way, 1, g], t_view(x, g), t_view(x, g), nxt)
        for h in (0, 1):
            across(0, h)

    def t_second():
        for way, nxt in ((1, right), (-1, left)):
            h = 0 if way == 1 else 1
            ref = t_view(up(x, -way, NX), h)
            net.arrived(tok_slots[way, 1, h], ref, nxt)
            net.send(tok_slots[way, 2, h], ref, ref, nxt)
            across((4 - way) % 4, h)

    def t_third():
        for way, nxt in ((1, right), (-1, left)):
            h = 1 if way == 1 else 0
            net.arrived(tok_slots[way, 1, h], t_view(up(x, -way, NX), h), nxt)
            across((4 - way) % 4, h)

    def t_fourth():
        for way, nxt in ((1, right), (-1, left)):
            h = 0 if way == 1 else 1
            net.arrived(tok_slots[way, 2, h], t_view(up(x, 2, NX), h), nxt)
            across(2, h)

    def t_last():
        for d in range(4):
            for h in (0, 1):
                net.arrived(chip_slots[d, h], t_view(up(x, d, NX), h, 1 - c), partner)
        for d in (1, 2, 3):
            net.arrived(sh_slots[d], sh_all.at[up(x, -d, NX)], at_axis("sp_1", up(x, d, NX)))

    todo += [(0.0, t_first), (4.6, t_second), (7.5, t_third), (11.0, t_fourth), (20.0, t_last)]

    yp_slots = {(e, d): net.slot() for e in (1, 2, 3) for d in range(4)}

    def w_piece(d):
        def act():
            xi = up(x, -d, NX)
            ref = w_all.at[z, xi, y]
            if d:
                net.arrived(in_slots[d], ref, at_axis("sp_1", xi))
            for e in (1, 2, 3):
                net.send(yp_slots[e, d], ref, ref, at_axis("fs", up(y, e, NY)))

        return act

    todo += [(0.1, w_piece(0)), (2.0, w_piece(1)), (2.1, w_piece(3)), (2.2, w_piece(2))]

    def w_ready(e):
        if e:
            for d in range(4):
                net.arrived(
                    yp_slots[e, d], w_all.at[z, up(x, -d, NX), up(y, -e, NY)], at_axis("fs", up(y, -e, NY))
                )

    z_ring(lambda i, e: w_all.at[i, :, up(y, -e, NY)], 4, w_ready, 2.4, 4.5)

    for _, act in sorted(todo, key=lambda item: item[0]):
        act()
    net.finish()


N_GATHER = 200


def gather(tok, wsl, own, shift):
    sds = jax.ShapeDtypeStruct
    hbm = pl.BlockSpec(memory_space=pltpu.HBM)
    vmem = pl.BlockSpec(memory_space=VM)
    return pl.pallas_call(
        gather_kernel,
        out_shape=(
            sds((NX, 2, T, 1024), BF),
            sds((NZ, NX, NY, 16, 384), BF),
            sds((NZ, NY, 16, 512), BF),
            sds((NX, 4, T), F32),
        ),
        in_specs=[hbm] * 4,
        out_specs=(vmem,) * 4,
        scratch_shapes=[
            VM((NX, 16, 384), BF),
            pltpu.SemaphoreType.DMA((5,)),
            pltpu.SemaphoreType.DMA((N_GATHER,)),
            pltpu.SemaphoreType.DMA((N_GATHER,)),
        ],
        compiler_params=pltpu.CompilerParams(collective_id=1, has_side_effects=True),
        name="gather",
    )(tok, wsl, own, shift)


def dot(a, b, ca=1, cb=0):
    return lax.dot_general(a, b, (((ca,), (cb,)), ((), ())), preferred_element_type=F32)


def bdot(a, b, ca=1, cb=0):
    return dot(a.astype(BF), b.astype(BF), ca, cb)


def split3(v):
    hi = v.astype(BF)
    rest = v - hi.astype(F32)
    mid = rest.astype(BF)
    return hi, mid, (rest - mid.astype(F32)).astype(BF)


def iota2(shape):
    return lax.broadcasted_iota(jnp.int32, shape, 0), lax.broadcasted_iota(jnp.int32, shape, 1)


def level_masks():
    i, j = iota2((T, T))
    masks = []
    h = 1
    while h < T:
        mid = (i // (2 * h)) * (2 * h) + h
        masks.append(((i >= mid) & (j >= mid) & (j < i)) | ((i < mid) & (j > i) & (j < mid)))
        h *= 2
    return masks + [j < i, j > i]


def own_head(x, array):
    out = array[:, :HD]
    for h in range(1, NX):
        out = jnp.where(x == h, array[:, h * HD : (h + 1) * HD], out)
    return out


def unit_solve(X, u, w, a, b, k, r, v):
    lane = slice(u * HD, (u + 1) * HD)
    i, j = iota2((T, T))
    eye = i == j
    right = jnp.concatenate([b, k], 0)
    left = jnp.concatenate([a, r * w], 0)
    diag = bdot(r, right, 1, 1)
    arb = jnp.where(eye, diag[:, :T], 0.0)
    ark = jnp.where(eye, diag[:, T:], 0.0)
    aak = jnp.zeros((T, T), F32)
    inv = jnp.where(eye, 1.0, 0.0)
    h, level = 1, 0
    while h < T:
        x = X[level * T : (level + 1) * T, lane]
        xx = jnp.concatenate([x, x], 0)
        score = bdot(left * xx, right * xx, 1, 1)
        mask = ((i // (2 * h)) == (j // (2 * h))) & ((i // h) % 2 == 1) & ((j // h) % 2 == 0)
        aab = jnp.where(mask, score[:T, :T], 0.0)
        aak = jnp.where(mask, score[:T, T:], aak)
        arb = jnp.where(mask, score[T:, :T], arb)
        ark = jnp.where(mask, score[T:, T:], ark)
        inv = inv + (aab if h == 1 else bdot(inv, bdot(aab, inv)))
        h, level = 2 * h, level + 1
    before = X[7 * T : 8 * T, lane]
    after = X[8 * T : 9 * T, lane]
    a_start, r_start = a * before, r * w * before
    b_end, k_end = b * after, k * after
    w_all = before[T - 1 : T] * w[T - 1 : T]
    uz = bdot(inv, jnp.concatenate([a_start, bdot(aak, v)], 1))
    writes = jnp.concatenate([uz, jnp.concatenate([jnp.zeros_like(v), v], 1)], 0)
    reads = bdot(jnp.concatenate([arb, ark], 1), writes)
    reads = reads + jnp.concatenate([r_start, jnp.zeros_like(r)], 1)
    i, j = iota2((HD, 2 * HD))
    passed = bdot(jnp.concatenate([b_end, k_end], 0).T, writes)
    passed = passed + jnp.where(i == j, jnp.concatenate([w_all, w_all], 1), 0.0)
    return reads, passed


def local_kernel(
    tok_all, gain, w_all, dd, rd, sh_all, params, dup, rup, reads_out, passed_out, total_out, conv_out, normed
):
    x = lax.axis_index("sp_1")
    rows = NX * T
    for u in range(NX):
        t0, t1 = tok_all[u, 0].astype(F32), tok_all[u, 1].astype(F32)
        square = jnp.sum(t0 * t0, -1, keepdims=True) + jnp.sum(t1 * t1, -1, keepdims=True)
        scale = lax.rsqrt(square / 2048.0 + RMS_EPS)
        normed[u * T : (u + 1) * T, :1024] = (t0 * scale * gain[:, :1024]).astype(BF)
        normed[u * T : (u + 1) * T, 1024:] = (t1 * scale * gain[:, 1024:]).astype(BF)
    n = normed[...]
    main = dot(n, w_all[...]).astype(BF)
    low = dot(n, jnp.concatenate([dd[...], rd[...]], 1))
    conv_out[...] = jnp.concatenate(
        [main[:, HD : 2 * HD].astype(F32) * main[:, 2 * HD : 3 * HD].astype(F32), main[:, :HD].astype(F32)], 1
    )
    recv = main[:, 3 * HD : 4 * HD].astype(F32)
    keys = main[:, 4 * HD : 5 * HD].astype(F32)
    vals = main[:, 5 * HD :].astype(F32)
    decay_low = jnp.tanh(low[:, :HD]).astype(BF)
    rate_low = low[:, HD:].astype(BF)
    table = own_head(x, params[...])
    pre = table[0:1] + dot(decay_low, own_head(x, dup[...]))
    rate = jax.nn.sigmoid(table[1:2] + dot(rate_low, own_head(x, rup[...])))
    base = -(jnp.maximum(-pre, 0.0) + jnp.log1p(jnp.exp(-jnp.abs(pre)))) - 0.5
    i, j = iota2((T, T))
    eye = i == j
    logs = []
    for u in range(NX):
        row = sh_all[u]
        mine = row[0:1]
        for h in range(1, NX):
            mine = jnp.where(x == h, row[h : h + 1], mine)
        column = jnp.sum(jnp.where(eye, mine, 0.0), -1, keepdims=True)
        logs.append(-jnp.exp(base[u * T : (u + 1) * T] + column))
    unit = keys * lax.rsqrt(jnp.sum(keys * keys, -1, keepdims=True) + UNIT_EPS)
    masks = jnp.concatenate([jnp.where(m, 1.0, 0.0) for m in level_masks()], 0).astype(BF)
    sums = sum(dot(masks, part) for part in split3(jnp.concatenate(logs, 1)))
    X = jnp.exp(sums)
    total = None
    i, j = iota2((HD, 2 * HD))
    for u in range(NX):
        s = slice(u * T, (u + 1) * T)
        reads, passed = unit_solve(
            X, u, jnp.exp(logs[u]), -unit[s], unit[s] * rate[s], keys[s] * rate[s], recv[s], vals[s]
        )
        reads_out[u] = reads
        passed_out[u] = passed
        if total is None:
            total = passed
        else:
            total = bdot(passed[:, :HD], total) + jnp.where(j >= HD, passed, 0.0)
    total_out[...] = total.astype(BF)


def local(tok_all, gain, w_all, dd, rd, sh_all, params, dup, rup):
    sds = jax.ShapeDtypeStruct
    vmem = pl.BlockSpec(memory_space=VM)
    return pl.pallas_call(
        local_kernel,
        out_shape=(
            sds((NX, T, 2 * HD), F32),
            sds((NX, HD, 2 * HD), F32),
            sds((HD, 2 * HD), BF),
            sds((NX * T, 2 * HD), F32),
        ),
        in_specs=[vmem] * 9,
        out_specs=(vmem,) * 4,
        scratch_shapes=[VM((NX * T, 2048), BF)],
        name="local",
    )(tok_all, gain, w_all, dd, rd, sh_all, params, dup, rup)


def finish_kernel(
    o_slab, reads, passed, total, conv, params, out,
    o_all, prefix, halo, state, pack, heads, to_partner, from_partner, own_part,
    local_sems, send_sems, recv_sems,
):
    z, x = lax.axis_index("sp_0"), lax.axis_index("sp_1")
    c = lax.axis_index("tp")

    def up(i, by, n):
        return lax.rem(i + by + n, n)

    mine = pltpu.make_async_copy(o_slab, o_all.at[:, x], local_sems.at[0])
    mine.start()
    barrier = pltpu.get_barrier_semaphore()
    peers = [at_axis("sp_1", up(x, d, NX)) for d in (1, 2, 3)]
    peers += [at_axis("sp_0", up(z, d, NZ)) for d in range(1, NZ)]
    peers += [at_axis("tp", 1 - c)]
    for peer in peers:
        pl.semaphore_signal(barrier, inc=1, device_id=peer, device_id_type=MESH)
    pl.semaphore_wait(barrier, len(peers))

    net = Copies(send_sems, recv_sems)
    net.used = 2 * NZ
    halo_slot = net.slot()
    send_slots = [net.slot() for _ in range(NZ)]

    def total_copy(to, d):
        return pltpu.make_async_remote_copy(
            src_ref=total, dst_ref=prefix.at[z], send_sem=send_sems.at[send_slots[d]],
            recv_sem=recv_sems.at[z], device_id=at_axis("sp_0", to), device_id_type=MESH,
        )

    for d in range(NZ - 1, 0, -1):

        @pl.when(z + d < NZ)
        def _(d=d):
            total_copy(lax.rem(z + d, NZ), d).start()

    tail = conv.at[pl.ds(NX * T - 8, 8)]

    @pl.when(z + 1 < NZ)
    def _():
        net.make(halo_slot, tail, halo, at_axis("sp_0", up(z, 1, NZ))).start()

    mine.wait()
    right, left = at_axis("sp_1", up(x, 1, NX)), at_axis("sp_1", up(x, -1, NX))
    slots = {(way, k, h): net.slot() for way in (1, -1) for k in (1, 2) for h in (0, 1)
             if k == 1 or (h == 0) == (way == 1)}

    def o_view(i, h):
        return o_all.at[pl.ds(4 * h, 4), i]

    for h in (0, 1):
        for way, nxt in ((1, right), (-1, left)):
            g = h if way == 1 else 1 - h
            net.send(slots[way, 1, g], o_view(x, g), o_view(x, g), nxt)

    table = own_head(x, params[...])

    @pl.when(z == 0)
    def _():
        halo[...] = jnp.zeros_like(halo)

    @pl.when(z > 0)
    def _():
        net.arrived(halo_slot, halo, at_axis("sp_0", up(z, -1, NZ)))

    for u in range(NX):
        s = slice(u * T, (u + 1) * T)
        before = halo[...] if u == 0 else conv[u * T - 8 : u * T]
        ext = jnp.concatenate([before, conv[s]], 0)[:, :HD]
        mixed = ext[6 : 6 + T] * table[3:4] + ext[7 : 7 + T] * table[4:5] + ext[8 : 8 + T] * table[5:6]
        pack[u, :, :HD] = (conv[s][:, HD:] * mixed).astype(BF)

    state[...] = jnp.zeros_like(state)
    for zz in range(NZ - 1):

        @pl.when(zz < z)
        def _(zz=zz):
            pltpu.make_async_remote_copy(
                src_ref=total, dst_ref=prefix.at[zz], send_sem=send_sems.at[0],
                recv_sem=recv_sems.at[zz], device_id=at_axis("sp_0", up(z, 1, NZ)), device_id_type=MESH,
            ).wait_recv()
            step = prefix[zz]
            state[...] = bdot(step[:, :HD], state[...]) + step[:, HD:].astype(F32)

    entering = state[...]
    for u in range(NX):
        got = reads[u]
        read = got[:, HD:] + bdot(got[:, :HD], entering)
        if u < NX - 1:
            step = passed[u]
            entering = bdot(step[:, :HD], entering) + step[:, HD:]
        centred = read - jnp.mean(read, -1, keepdims=True)
        variance = jnp.mean(centred * centred, -1, keepdims=True)
        pack[u, :, HD:] = (centred * lax.rsqrt(variance + GROUP_EPS) * table[2:3]).astype(BF)

    for way, nxt in ((1, right), (-1, left)):
        h = 0 if way == 1 else 1
        ref = o_view(up(x, -way, NX), h)
        net.arrived(slots[way, 1, h], ref, nxt)
        net.send(slots[way, 2, h], ref, ref, nxt)

    head_slots = [None] + [net.slot() for _ in range(3)]
    for d in (1, 2, 3):
        to = up(x, d, NX)
        net.send(head_slots[d], pack.at[to], heads.at[x], at_axis("sp_1", to))
    heads[x] = pack[x]
    for d in (1, 2, 3):
        net.arrived(head_slots[d], heads.at[up(x, -d, NX)], at_axis("sp_1", up(x, d, NX)))
    for way, nxt in ((1, right), (-1, left)):
        h = 0 if way == 1 else 1
        net.arrived(slots[way, 1, 1 - h], o_view(up(x, -way, NX), 1 - h), nxt)
        net.arrived(slots[way, 2, h], o_view(up(x, 2, NX), h), nxt)

    theirs = pl.multiple_of((1 - c) * 64, 64)
    ours = pl.multiple_of(c * 64, 64)
    lhs = jnp.concatenate(
        [
            jnp.concatenate([heads[h, pl.ds(theirs, 64), :] for h in range(NX)], 1),
            jnp.concatenate([heads[h, pl.ds(ours, 64), :] for h in range(NX)], 1),
        ],
        0,
    )
    chip_slots = [net.slot() for _ in range(NZ)]
    partner = at_axis("tp", 1 - c)
    for zz in range(NZ):
        part = dot(lhs, o_all[zz].reshape(256, 512), 1, 1).astype(BF)
        to_partner[zz] = part[:64]
        own_part[zz] = part[64:]
        net.send(chip_slots[zz], to_partner.at[zz], from_partner.at[zz], partner)
    for zz in range(NZ):
        net.arrived(chip_slots[zz], from_partner.at[zz], partner)
        out[:, zz * 256 : (zz + 1) * 256] = (
            own_part[zz].astype(F32) + from_partner[zz].astype(F32)
        ).astype(BF)
    net.finish()
    for d in range(NZ - 1, 0, -1):

        @pl.when(z + d < NZ)
        def _(d=d):
            total_copy(lax.rem(z + d, NZ), d).wait_send()

    @pl.when(z + 1 < NZ)
    def _():
        net.make(halo_slot, tail, halo, at_axis("sp_0", up(z, 1, NZ))).wait_send()


def finish(o_slab, reads, passed, total, conv, params):
    hbm = pl.BlockSpec(memory_space=pltpu.HBM)
    vmem = pl.BlockSpec(memory_space=VM)
    return pl.pallas_call(
        finish_kernel,
        out_shape=jax.ShapeDtypeStruct((64, 2048), BF),
        in_specs=[hbm] + [vmem] * 5,
        out_specs=vmem,
        scratch_shapes=[
            VM((NZ, NX, NY, 16, 512), BF),
            VM((NZ, HD, 2 * HD), BF),
            VM((8, 2 * HD), F32),
            VM((HD, HD), F32),
            VM((NX, T, 2 * HD), BF),
            VM((NX, T, 2 * HD), BF),
            VM((NZ, 64, 256), BF),
            VM((NZ, 64, 256), BF),
            VM((NZ, 64, 256), BF),
            pltpu.SemaphoreType.DMA((1,)),
            pltpu.SemaphoreType.DMA((64,)),
            pltpu.SemaphoreType.DMA((64,)),
        ],
        compiler_params=pltpu.CompilerParams(collective_id=2, has_side_effects=True),
        name="finish",
    )(o_slab, reads, passed, total, conv, params)


def body(
    tokens, norm_gain, conv_gate_out, conv_gate_in, conv_value, conv_taps, recv_weight, key_weight,
    value_weight, decay_base, decay_down, decay_up, decay_shift, rate_base, rate_down, rate_up,
    head_gain, out_conv, out_state,
):
    wsl = jnp.stack([conv_gate_out, conv_gate_in, conv_value, recv_weight, key_weight, value_weight], 1)
    wsl = wsl.reshape(16, 6, NX, HD).transpose(2, 0, 1, 3).reshape(NX, 16, 6 * HD)
    own = jnp.stack([out_conv.reshape(NX, HD, 16), out_state.reshape(NX, HD, 16)], 1)
    own = own.reshape(8 * HD, 16).T
    shift = decay_shift.reshape(T, NX).T
    params = jnp.concatenate(
        [decay_base[None], rate_base[None], head_gain[None], conv_taps, jnp.zeros((2, 256), F32)], 0
    )
    tok_all, w_all, o_slab, sh_all = gather(tokens.reshape(T, 1024), wsl, own, shift)
    reads, passed, total, conv = local(
        tok_all, norm_gain.reshape(1, 2048), w_all.reshape(2048, 384), decay_down, rate_down, sh_all,
        params, decay_up, rate_up,
    )
    return finish(o_slab, reads, passed, total, conv, params).reshape(1, 64, 2048)


def solution(mesh):
    torus = Mesh(
        mesh.devices.reshape(NZ, NX, mesh.shape["fs"], mesh.shape["tp"]), ("sp_0", "sp_1", "fs", "tp")
    )
    placed = (
        P("fs", SP, "tp"), P(), P(SP_FS, "tp"), P(SP_FS, "tp"), P(SP_FS, "tp"), P(None, "tp"),
        P(SP_FS, "tp"), P(SP_FS, "tp"), P(SP_FS, "tp"), P("tp"), P(), P(None, "tp"), P("fs", SP, "tp"),
        P("tp"), P(), P(None, "tp"), P("tp"), P("tp", SP_FS), P("tp", SP_FS),
    )
    return jax.shard_map(
        body, mesh=torus, in_specs=placed, out_specs=P("fs", SP_TP, None), check_vma=False
    )
```

time: 287 us -> 101 us (0.35)
  blocking collectives: 104 us -> 0 us
  Pallas kernels: 0 us -> 87 us
  waiting for transfers between devices: 70.2 us -> 0 us
  other arithmetic: 42.4 us -> 0.1 us
  matrix products: 37.3 us -> 0 us
  between operations: 13.9 us -> 0.1 us
  starting transfers between devices: 9.69 us -> 0 us
  local copies, waits for them, and re-layouts: 8.72 us -> 13.5 us
    pallas_call x0 -> x3, Pallas kernels: none -> 87 us  [the longest x1 37.2 us: gather(): pl.pallas_call(gather_kernel, out_shape=(sds((NX, 2, T, 1024), BF), sds((...]
    all_gather x6 -> x0, blocking collectives: 81.7 us -> none  [the longest x4 60.4 us: entering_2(): lax.all_gather(part.astype(kind), axis)]
    all_gather x2 -> x0, waiting for transfers between devices: 70.2 us -> none  [the longest x1 70.2 us: in_one_piece(): result = lax.all_gather(both, axis, axis=dim, tiled=True)]
    another operation x24 -> x1, other arithmetic: 40.2 us -> 0.1 us  [body(): jnp.stack([out_conv.reshape(NX, HD, 16), out_state.reshape(NX, HD, 16)], 1)]
    dot_general x71 -> x0, matrix products: 36.1 us -> none  [the longest x5 7.87 us: fold_rows(): jnp.dot(normed, pieces[member], preferred_element_type=jnp.float32)]
    all_to_all x1 -> x0, blocking collectives: 21.8 us -> none  [sum_at_owner(): lax.all_to_all(pieces, axis, split_axis=0, concat_axis=0, tiled=True)]
    all_to_all x1 -> x0, starting transfers between devices: 8.02 us -> none  [sent_to_all(): return lax.all_to_all(copies, axis, split_axis=0, concat_axis=0, tiled=True)]
    another operation x0 -> x15, local copies, waits for them, and re-layouts: none -> 6.76 us  [the longest x13 5.19 us: body(): jnp.stack([conv_gate_out, conv_gate_in, conv_value, recv_weight, key_weig...]
  transfers between devices with their start and end apart: 4 -> 0, of which waited for: 1 -> 0; matrix products, arithmetic and copies ran while one was open for 28% -> 0% of each run, Pallas kernels for 0% -> 0%
where the time goes in v1:
time: 101 us
  Pallas kernels  87 us (86%)
  local copies, waits for them, and re-layouts  13.5 us (13%)
    pallas_call x1, Pallas kernels, gather(): pl.pallas_call(gather_kernel, out_shape=(sds((NX, 2, T, 1024), BF), sds((...  37.2 us
    pallas_call x1, Pallas kernels, finish(): pl.pallas_call(finish_kernel, out_shape=jax.ShapeDtypeStruct((64, 2048),...  33.6 us
    pallas_call x1, Pallas kernels, local(): pl.pallas_call(local_kernel, out_shape=(sds((NX, T, 2 * HD), F32), sds((N...  16.2 us
    another operation x13, local copies, waits for them, and re-layouts, body(): jnp.stack([conv_gate_out, conv_gate_in, conv_value, recv_weight, key_weig...  5.19 us
    unnamed x13, local copies, waits for them, and re-layouts  4.66 us

profile of v1, /device:TPU:1, one launch (start us, length us, event | category | flops | bytes accessed | tf_op | source)
XLA Modules:
  0.0 100.7 jit_solution(1553959343070549146)
XLA Ops:
  0.0 0.0 copy-start
  0.0 0.0 copy-start.2
  0.0 0.0 copy-start.3
  0.0 0.0 copy-start.4
  0.0 0.0 copy-start.1
  0.0 0.8 stack.24
  0.9 0.8 stack.25
  1.7 0.8 stack.26
  2.5 0.8 stack.27
  3.3 0.8 stack.28
  4.1 0.8 stack.29
  5.0 0.3 stack.30
  5.3 0.8 reshape.35.wsl
  6.0 0.8 stack_reshape.9
  6.8 0.8 stack_reshape.8
  7.6 0.1 pad_maximum_fusion
  7.7 0.7 reshape.36
  8.4 37.2 %gather.1 = (bf16[4,2,128,1024]{3,2,1,0:T(8,128)(2,1)}, bf16[8,4,4,16,384]{4,3,2,1,0:T(8,128)(2,1)}, bf16[8,4,16,512]{3,2,1,0:T(8,128)(2,1)}, f32[4,4,128]{2,1,0:T(4,128)}) custom-call(bf16[128,1024]{1,0:T(8,128)(2,1)} %bitcast.21, bf16[4,16,384]{2,1,0:T(8,128)(2,1)} %reshape.35.wsl, bf16[16,512]{1,0:T(8,128)(2,1)} %bitcast.22, f32[4,128]{1,0:T(4,128)} %bitcast.24), custom_call_target="tpu_custom_call" | custom-call | tf_op jit(solution)/shard_map/gather/pallas_call | solution.py:253
  45.6 2.0 %copy.38.dd = bf16[2048,64]{1,0:T(8,128)(2,1)} copy(bf16[2048,64]{0,1:T(8,128)(2,1)} %param.29) | data formatting | bytes 524288 | tf_op args[10]
  47.5 0.0 copy-done
  47.5 1.0 %copy.39.rd = bf16[2048,64]{1,0:T(8,128)(2,1)} copy(bf16[2048,64]{0,1:T(8,128)(2,1)S(1)} %copy-done) | data formatting | bytes 524288 | tf_op args[14]
  48.6 0.0 copy-done.2
  48.6 0.0 copy-done.3
  48.6 0.0 copy-done.4
  48.6 0.0 copy-done.1
  48.6 0.6 concatenate.4.params
  49.2 16.2 %local.1 = (f32[4,128,128]{2,1,0:T(8,128)}, f32[4,64,128]{2,1,0:T(8,128)}, bf16[64,128]{1,0:T(8,128)(2,1)}, f32[512,128]{1,0:T(8,128)}) custom-call(bf16[4,2,128,1024]{3,2,1,0:T(8,128)(2,1)} %get-tuple-element.14.tok_all, f32[1,2048]{1,0:T(1,128)} %bitcast.23, bf16[2048,384]{1,0:T(8,128)(2,1)} %bitcast.18, bf16[2048,64]{1,0:T(8,128)(2,1)} %copy.38.dd, ...), custom_call_target="tpu_custom_call" | custom-call | tf_op jit(solution)/shard_map/local/pallas_call | solution.py:408
  65.4 33.6 %finish.1 = bf16[64,2048]{1,0:T(8,128)(2,1)} custom-call(bf16[8,4,16,512]{3,2,1,0:T(8,128)(2,1)} %get-tuple-element.13.o_slab, f32[4,128,128]{2,1,0:T(8,128)} %get-tuple-element.17.reads, f32[4,64,128]{2,1,0:T(8,128)} %get-tuple-element.18.passed, bf16[64,128]{1,0:T(8,128)(2,1)} %get-tuple-element.19.total, f32[512,128]{1,0:T(8,128)} %get-tuple-element.20.conv, ...), custom_call_target="tpu_custom_call" | custom-call | tf_op jit(solution)/shard_map/finish/pallas_call | solution.py:574
  99.0 1.7 %copy.41 = bf16[1,64,2048]{2,1,0:T(8,128)(2,1)} copy(bf16[1,64,2048]{2,1,0:T(8,128)(2,1)} %bitcast.19) | data formatting | bytes 524288
  (7 shorter events, 0.2 us)
Async XLA Ops:
  0.0 47.5 %copy-start = (bf16[2048,64]{0,1:T(8,128)(2,1)S(1)}, bf16[2048,64]{0,1:T(8,128)(2,1)}, u32[]{:S(2)}) copy-start(bf16[2048,64]{0,1:T(8,128)(2,1)} %param.33) | copy-start | bytes 786436
  0.0 48.6 %copy-start.2 = (f32[256]{0:T(256)S(1)}, f32[256]{0:T(256)}, u32[]{:S(2)}) copy-start(f32[256]{0:T(256)} %param.28) | copy-start | bytes 3076
  0.0 48.6 %copy-start.3 = (f32[256]{0:T(256)S(1)}, f32[256]{0:T(256)}, u32[]{:S(2)}) copy-start(f32[256]{0:T(256)} %param.32) | copy-start | bytes 3076
  0.0 48.6 %copy-start.4 = (f32[256]{0:T(256)S(1)}, f32[256]{0:T(256)}, u32[]{:S(2)}) copy-start(f32[256]{0:T(256)} %param.35) | copy-start | bytes 3076
  0.0 48.5 %copy-start.1 = (f32[3,256]{1,0:T(4,128)S(1)}, f32[3,256]{1,0:T(4,128)}, u32[]{:S(2)}) copy-start(f32[3,256]{1,0:T(4,128)} %param.24) | copy-start | bytes 9220
